TPU v7x, 32 devices: a whole 2x2x4 slice. The times are simulated.
32 devices in a mesh: gr: 2 (over x), fs: 8 (over z, y), tp: 2 (over core).
Axes of the slice: x: 2, y: 2, z: 4, core: 2. Of those that a mesh axis runs over, the one named last changes fastest.
Arguments:
- tokens: bfloat16 [4096, 2048], P(('gr', 'fs', 'tp')), may hold values from -6 to 6
- norm_gain: float32 [2048], P(('gr', 'fs')), may hold values from 0.1 to 1.9
- up_weight: float32 [2048, 8192], P(('gr', 'fs'), 'tp'), may hold values from -0.125 to 0.125
- down_weight: float32 [8192, 2048], P(('gr', 'fs'), 'tp'), may hold values from -0.0625 to 0.0625
Outputs:
- served: bfloat16 [4096, 2048], P(('gr', 'fs', 'tp'))
- serve_up: bfloat16 [2048, 8192], P(None, 'fs')
- serve_down: bfloat16 [8192, 2048], P('fs')
All inputs are finite; a program needn't handle non-finite values.
Results may differ from a plain program's by a relative error of at most 0.017.
Values may be sent and summed in bfloat16 or wider, within the bound.
A program may use at most 64 MiB of HBM per device.

v0:
```python
import jax
import jax.numpy as jnp
from jax import lax
from jax.sharding import PartitionSpec as P


def body(tokens, norm_gain, up_weight, down_weight):
    groups = lax.axis_size("gr")
    shards = lax.axis_size("fs")
    segment = down_weight.shape[0]
    own_rows = up_weight.shape[0]
    up_local = (norm_gain[:, None] * up_weight).astype(jnp.bfloat16)
    down_local = down_weight.astype(jnp.bfloat16)
    up_cols, down_cols = (
        lax.all_gather(up_local, "tp", axis=1, tiled=True),
        lax.all_gather(down_local, "tp", axis=1, tiled=True),
    )
    width = up_cols.shape[1]
    up_sorted = (
        up_cols.reshape(own_rows, groups, shards, segment)
        .transpose(0, 2, 1, 3)
        .reshape(own_rows, width)
    )
    up_mine = lax.all_to_all(up_sorted, "fs", split_axis=1, concat_axis=0, tiled=True)
    serve_up, serve_down = (
        lax.all_gather(up_mine, "gr", axis=0, tiled=True),
        lax.all_gather(down_cols, "gr", axis=0, tiled=True),
    )
    values = tokens.astype(jnp.float32)
    normed = (values * lax.rsqrt(jnp.mean(values * values, axis=1, keepdims=True) + 1e-06)).astype(
        jnp.bfloat16
    )
    product = jnp.dot(
        lax.all_gather(normed, "fs", axis=0, tiled=True),
        serve_up,
        preferred_element_type=jnp.float32,
    )
    hidden = jnp.square(jax.nn.relu(product)).astype(jnp.bfloat16)
    part = jnp.dot(hidden, serve_down, preferred_element_type=jnp.float32).astype(jnp.bfloat16)
    part = lax.optimization_barrier(part)
    summed = lax.psum_scatter(
        part.astype(jnp.float32).astype(jnp.bfloat16), "fs", scatter_dimension=0, tiled=True
    )
    return (summed, serve_up, serve_down)


def solution(mesh):
    return jax.shard_map(
        body,
        mesh=mesh,
        in_specs=(
            P(("gr", "fs", "tp"), None),
            P(("gr", "fs")),
            P(("gr", "fs"), "tp"),
            P(("gr", "fs"), "tp"),
        ),
        out_specs=(P(("gr", "fs", "tp"), None), P(None, "fs"), P("fs", None)),
        check_vma=False,
    )
```

profile of v0, /device:TPU:0, one launch (start us, length us, event | category | flops | bytes accessed | tf_op | source)
XLA Modules:
  0.0 345.5 jit_solution(10217558467831381124)
XLA Ops:
  7.2 0.0 copy-start.1
  7.2 0.0 copy-start.3
  7.2 0.0 all-gather.12.cloned.1.call-start
  7.2 2.9 convert_element_type.24
  10.1 0.0 copy-start.2
  10.1 0.0 all-gather.12.cloned.1.call-update
  10.1 0.0 all-gather.8.cloned.1.call-start
  10.2 0.0 copy-done.1
  10.2 0.0 copy-done.3
  10.2 1.2 multiply_convert_fusion.1
  11.4 0.0 all-gather.8.cloned.1.call-update
  11.4 0.0 all-gather.14.cloned.1.call-start
  11.4 12.1 %all-gather.12.cloned.1.call-done = bf16[512,2048]{1,0:T(8,128)(2,1)} async-done(((bf16[512,1024]{1,0:T(8,128)(2,1)}), bf16[512,2048]{1,0:T(8,128)(2,1)}) %all-gather.12.cloned.1.call-update) | async-done | bytes 2097168 | tf_op jit(solution)/shard_map/all_gather | solution.py:16
  23.6 0.0 all-gather.14.cloned.1.call-update
  23.6 0.0 all-gather.6.cloned.1.call-start
  23.6 0.0 copy-done.2
  23.7 0.2 fusion
  23.9 1.0 fusion.1
  24.8 0.0 all-gather.6.cloned.1.call-update
  24.8 0.0 all-gather.10.cloned.1.call-start
  24.9 12.6 %all-gather.8.cloned.1.call-done = bf16[128,8192]{1,0:T(8,128)(2,1)} async-done(((bf16[128,4096]{1,0:T(8,128)(2,1)}), bf16[128,8192]{1,0:T(8,128)(2,1)}) %all-gather.8.cloned.1.call-update) | async-done | bytes 2097168 | tf_op jit(solution)/shard_map/all_gather | solution.py:15
  37.5 2.4 copy.8
  39.9 1.6 copy.7
  41.5 2.7 all_to_all.14
  44.2 54.5 %all_to_all.19 = bf16[128,8,1024]{2,0,1:T(8,128)(2,1)} all-to-all(bf16[128,8,1024]{2,0,1:T(8,128)(2,1)} %all_to_all.14), channel_id=1, replica_groups=mesh['gr'=2,'fs'=8,'tp'=2] {'fs'}, dimensions={1} | all-to-all | bytes 4194304 | tf_op jit(solution)/shard_map/all_to_all | solution.py:24
  98.8 0.0 all-gather.10.cloned.1.call-update
  98.8 0.0 reduce-scatter.2.cloned.1.call-start
  98.8 0.0 all-gather.14.cloned.1.call-done
  98.9 73.5 %all-gather.6.cloned.1.call-done = bf16[1024,2048]{1,0:T(8,128)(2,1)} async-done(((bf16[128,2048]{1,0:T(8,128)(2,1)}), bf16[1024,2048]{1,0:T(8,128)(2,1)}) %all-gather.6.cloned.1.call-update) | async-done | bytes 4194320 | tf_op jit(solution)/shard_map/all_gather | solution.py:34
  172.3 56.7 %all-gather.10.cloned.1.call-done = bf16[2048,1024]{1,0:T(8,128)(2,1)} async-done(((bf16[1024,1024]{1,0:T(8,128)(2,1)}), bf16[2048,1024]{1,0:T(8,128)(2,1)}) %all-gather.10.cloned.1.call-update) | async-done | bytes 4194320 | tf_op jit(solution)/shard_map/all_gather | solution.py:26
  229.0 14.4 %convolution_convert_fusion = bf16[1024,2048]{1,0:T(8,128)(2,1)} fusion(bf16[1024,2048]{1,0:T(8,128)(2,1)} %all-gather.14.cloned.1.call-done, bf16[1024,2048]{1,0:T(8,128)(2,1)} %all-gather.6.cloned.1.call-done, bf16[2048,1024]{1,0:T(8,128)(2,1)} %all-gather.10.cloned.1.call-done), kind=kOutput, calls=%fused_computation.1 | convolution fusion | flops 8595177472 | bytes 16777216 | tf_op jit(solution)/shard_map/dot_general | solution.py:39
  243.4 0.0 reduce-scatter.2.cloned.1.call-update
  243.4 88.5 %reduce-scatter.2.cloned.1.call-done = bf16[128,2048]{1,0:T(8,128)(2,1)} async-done(((bf16[1024,2048]{1,0:T(8,128)(2,1)}), bf16[128,2048]{1,0:T(8,128)(2,1)}) %reduce-scatter.2.cloned.1.call-update) | async-done | bytes 524304 | tf_op jit(solution)/shard_map/reduce_scatter | solution.py:41
  331.9 0.0 copy-start
  331.9 4.8 %copy.11 = bf16[2048,1024]{1,0:T(8,128)(2,1)} copy(bf16[2048,1024]{1,0:T(8,128)(2,1)} %all-gather.10.cloned.1.call-done) | data formatting | bytes 8388608
  336.7 0.0 copy-done
  336.7 2.0 copy.12
  (1 shorter events, 0.0 us)
Async XLA Ops:
  7.2 3.0 copy-start.1
  7.2 3.0 copy-start.3
  7.2 16.4 %all-gather.12.cloned.1.call-start = ((), (), s32[]{:S(2)}) async-start(), calls=%async_computation.5 | async-start | bytes 3145728 | tf_op jit(solution)/shard_map/all_gather | solution.py:16
  10.1 13.6 %copy-start.2 = (bf16[128,2048]{1,0:T(8,128)(2,1)S(1)}, bf16[128,2048]{1,0:T(8,128)(2,1)}, u32[]{:S(2)}) copy-start(bf16[128,2048]{1,0:T(8,128)(2,1)} %param.4) | copy-start | bytes 1572868
  10.1 27.4 %all-gather.8.cloned.1.call-start = ((), (), s32[]{:S(2)}) async-start(), calls=%async_computation.3 | async-start | bytes 3145728 | tf_op jit(solution)/shard_map/all_gather | solution.py:15
  11.4 87.5 %all-gather.14.cloned.1.call-start = ((), (), s32[]{:S(2)}) async-start(), calls=%async_computation.6 | async-start | bytes 6291456 | tf_op jit(solution)/shard_map/all_gather | solution.py:27
  23.6 148.7 %all-gather.6.cloned.1.call-start = ((), (), s32[]{:S(2)}) async-start(), calls=%async_computation.2 | async-start | bytes 4718592 | tf_op jit(solution)/shard_map/all_gather | solution.py:34
  24.8 204.2 %all-gather.10.cloned.1.call-start = ((), (), s32[]{:S(2)}) async-start(), calls=%async_computation.4 | async-start | bytes 6291456 | tf_op jit(solution)/shard_map/all_gather | solution.py:26
  98.8 233.1 %reduce-scatter.2.cloned.1.call-start = ((), (), s32[]{:S(2)}) async-start(), calls=%async_computation.7 | async-start | bytes 4718592 | tf_op jit(solution)/shard_map/reduce_scatter | solution.py:41
  331.9 4.8 %copy-start = (bf16[1024,2048]{1,0:T(8,128)(2,1)S(1)}, bf16[1024,2048]{1,0:T(8,128)(2,1)}, u32[]{:S(2)}) copy-start(bf16[1024,2048]{1,0:T(8,128)(2,1)} %all-gather.14.cloned.1.call-done) | copy-start | bytes 12582916
Sparse Core Ops, SparseCore 0:
  10.2 13.2 all-gather.11
  25.7 11.7 all-gather.7
  39.0 57.8 all-gather.13
  99.5 72.7 all-gather.5
  173.7 55.2 all-gather.9
  243.5 88.2 reduce-scatter.1
where the time goes:
time: 346 us
  waiting for transfers between devices  243 us (70%)
  blocking collectives  54.5 us (16%)
  matrix products  14.4 us (4%)
  between operations  14.2 us (4%)
  local copies, waits for them, and re-layouts  13.6 us (4%)
  other arithmetic  5.2 us (2%)
    reduce_scatter x1, waiting for transfers between devices, body(): lax.psum_scatter(part.astype(jnp.float32).astype(jnp.bfloat16), 'fs', sca...  88.5 us
    all_gather x1, waiting for transfers between devices, body(): lax.all_gather(normed, 'fs', axis=0, tiled=True)  73.5 us
    all_gather x1, waiting for transfers between devices, body(): lax.all_gather(up_mine, 'gr', axis=0, tiled=True)  56.7 us
    all_to_all x1, blocking collectives, body(): lax.all_to_all(up_sorted, 'fs', split_axis=1, concat_axis=0, tiled=True)  54.5 us
    dot_general x1, matrix products, body(): jnp.dot(hidden, serve_down, preferred_element_type=jnp.float32)  14.4 us
    all_gather x1, waiting for transfers between devices, body(): lax.all_gather(up_local, 'tp', axis=1, tiled=True)  12.6 us
    all_gather x1, waiting for transfers between devices, body(): lax.all_gather(down_local, 'tp', axis=1, tiled=True)  12.1 us
    unnamed x11, local copies, waits for them, and re-layouts  9.26 us
  transfers between devices with their start and end apart: 6, of which 5 were waited for; matrix products, arithmetic and copies ran while one was open for 2% of the time, Pallas kernels for 0%

commit v1 on v0

--- a/solution.py
+++ b/solution.py
@@ -23,7 +23,9 @@
     )
     up_mine = lax.all_to_all(up_sorted, "fs", split_axis=1, concat_axis=0, tiled=True)
     serve_up, serve_down = (
-        lax.all_gather(up_mine, "gr", axis=0, tiled=True),
+        jnp.concatenate(
+            lax.all_to_all(jnp.stack([up_mine] * lax.axis_size("gr")), "gr", 0, 0), axis=0
+        ),
         lax.all_gather(down_cols, "gr", axis=0, tiled=True),
     )
     values = tokens.astype(jnp.float32)

time: 346 us -> 287 us (0.83)
  waiting for transfers between devices: 243 us -> 178 us
  starting transfers between devices: 0.24 us -> 5.84 us
    all_gather x1 -> x0, waiting for transfers between devices: 56.7 us -> none  [body(): lax.all_gather(up_mine, 'gr', axis=0, tiled=True)]
    all_gather x1, waiting for transfers between devices: 73.5 us -> 67.8 us  [body(): lax.all_gather(normed, 'fs', axis=0, tiled=True)]
    all_to_all x0 -> x1, starting transfers between devices: none -> 5.64 us  [body(): lax.all_to_all(jnp.stack([up_mine] * lax.axis_size('gr')), 'gr', 0, 0)]
    unnamed x11 -> x9, local copies, waits for them, and re-layouts: 9.26 us -> 8.75 us
  transfers between devices with their start and end apart: 6 -> 6, of which waited for: 5 -> 4; matrix products, arithmetic and copies ran while one was open for 2% -> 4% of each run, Pallas kernels for 0% -> 0%
where the time goes in v1:
time: 287 us
  waiting for transfers between devices  178 us (62%)
  blocking collectives  54.3 us (19%)
  matrix products  14.4 us (5%)
  between operations  13.9 us (5%)
  local copies, waits for them, and re-layouts  13.4 us (5%)
  other arithmetic  7.33 us (3%)
  starting transfers between devices  5.84 us (2%)
    reduce_scatter x1, waiting for transfers between devices, body(): lax.psum_scatter(part.astype(jnp.float32).astype(jnp.bfloat16), 'fs', sca...  87 us
    all_gather x1, waiting for transfers between devices, body(): lax.all_gather(normed, 'fs', axis=0, tiled=True)  67.8 us
    all_to_all x1, blocking collectives, body(): lax.all_to_all(up_sorted, 'fs', split_axis=1, concat_axis=0, tiled=True)  54.3 us
    dot_general x1, matrix products, body(): jnp.dot(hidden, serve_down, preferred_element_type=jnp.float32)  14.4 us
    all_gather x1, waiting for transfers between devices, body(): lax.all_gather(up_local, 'tp', axis=1, tiled=True)  12.6 us
    all_gather x1, waiting for transfers between devices, body(): lax.all_gather(down_local, 'tp', axis=1, tiled=True)  10.3 us
    unnamed x9, local copies, waits for them, and re-layouts  8.75 us
  transfers between devices with their start and end apart: 6, of which 4 were waited for; matrix products, arithmetic and copies ran while one was open for 4% of the time, Pallas kernels for 0%

profile of v1, /device:TPU:0, one launch (start us, length us, event | category | flops | bytes accessed | tf_op | source)
XLA Modules:
  0.0 286.9 jit_solution(16189830074422669262)
XLA Ops:
  7.2 0.0 copy-start.2
  7.2 0.0 all-gather.9.cloned.1.call-start
  7.2 2.7 convert_element_type.24
  9.9 0.0 all-gather.9.cloned.1.call-update
  10.0 0.0 all-gather.7.cloned.1.call-start
  10.0 1.9 copy.7
  11.9 0.0 copy-done.2
  12.0 0.0 copy-start.1
  12.0 1.1 multiply_convert_fusion.1
  13.0 0.0 all-gather.7.cloned.1.call-update
  13.1 0.0 all-gather.11.cloned.1.call-start
  13.1 10.3 %all-gather.9.cloned.1.call-done = bf16[512,2048]{1,0:T(8,128)(2,1)} async-done(((bf16[512,1024]{1,0:T(8,128)(2,1)}), bf16[512,2048]{1,0:T(8,128)(2,1)}) %all-gather.9.cloned.1.call-update) | async-done | bytes 2097168 | tf_op jit(solution)/shard_map/all_gather | solution.py:16
  23.4 0.0 all-gather.11.cloned.1.call-update
  23.5 0.0 all-gather.5.cloned.1.call-start
  23.5 0.0 copy-done.1
  23.5 0.2 fusion
  23.7 1.0 fusion.1
  24.7 0.0 all-gather.5.cloned.1.call-update
  24.7 12.6 %all-gather.7.cloned.1.call-done = bf16[128,8192]{0,1:T(8,128)(2,1)} async-done(((bf16[128,4096]{0,1:T(8,128)(2,1)}), bf16[128,8192]{0,1:T(8,128)(2,1)}) %all-gather.7.cloned.1.call-update) | async-done | bytes 2097168 | tf_op jit(solution)/shard_map/all_gather | solution.py:15
  37.3 1.7 copy.8
  39.1 54.3 %all_to_all.21 = bf16[128,8,1024]{0,2,1:T(8,128)(2,1)} all-to-all(bf16[128,8,1024]{0,2,1:T(8,128)(2,1)S(1)} %bitcast.11), channel_id=1, replica_groups=mesh['gr'=2,'fs'=8,'tp'=2] {'fs'}, dimensions={1} | all-to-all | bytes 4194304 | tf_op jit(solution)/shard_map/all_to_all | solution.py:24
  93.4 2.9 copy.9
  96.3 2.4 pad_maximum_fusion
  98.7 5.6 %all-to-all-start.1 = ((bf16[2,1024,1024]{2,1,0:T(8,128)(2,1)}), bf16[2,1024,1024]{2,1,0:T(8,128)(2,1)}, u32[]{:S(2)}, u32[]{:S(2)}) async-start(bf16[2,1024,1024]{2,1,0:T(8,128)(2,1)} %pad_maximum_fusion), calls=%async_computation.1 | async-start | bytes 8388608 | tf_op jit(solution)/shard_map/all_to_all | solution.py:27
  104.3 0.0 reduce-scatter.2.cloned.1.call-start
  104.4 0.0 all-gather.11.cloned.1.call-done
  104.4 67.8 %all-gather.5.cloned.1.call-done = bf16[1024,2048]{1,0:T(8,128)(2,1)} async-done(((bf16[128,2048]{1,0:T(8,128)(2,1)}), bf16[1024,2048]{1,0:T(8,128)(2,1)}) %all-gather.5.cloned.1.call-update) | async-done | bytes 4194320 | tf_op jit(solution)/shard_map/all_gather | solution.py:36
  172.2 0.0 all-to-all-done.1
  172.2 14.4 %convolution_convert_fusion = bf16[1024,2048]{1,0:T(8,128)(2,1)} fusion(bf16[1024,2048]{1,0:T(8,128)(2,1)} %all-gather.11.cloned.1.call-done, bf16[1024,2048]{1,0:T(8,128)(2,1)} %all-gather.5.cloned.1.call-done, bf16[2048,1024]{1,0:T(8,128)(2,1)} %bitcast.5), kind=kOutput, calls=%fused_computation.2 | convolution fusion | flops 8595177472 | bytes 16777216 | tf_op jit(solution)/shard_map/dot_general | solution.py:41
  186.6 0.0 reduce-scatter.2.cloned.1.call-update
  186.6 87.0 %reduce-scatter.2.cloned.1.call-done = bf16[128,2048]{1,0:T(8,128)(2,1)} async-done(((bf16[1024,2048]{1,0:T(8,128)(2,1)}), bf16[128,2048]{1,0:T(8,128)(2,1)}) %reduce-scatter.2.cloned.1.call-update) | async-done | bytes 524304 | tf_op jit(solution)/shard_map/reduce_scatter | solution.py:43
  273.6 0.0 copy-start
  273.6 4.8 %copy.12 = bf16[2048,1024]{1,0:T(8,128)(2,1)} copy(bf16[2048,1024]{1,0:T(8,128)(2,1)} %bitcast.5) | data formatting | bytes 8388608
  278.4 0.0 copy-done
  278.4 2.0 copy.13
  (1 shorter events, 0.0 us)
Async XLA Ops:
  7.2 4.8 %copy-start.2 = (f32[128]{0:T(128)S(1)}, f32[128]{0:T(128)}, u32[]{:S(2)}) copy-start(f32[128]{0:T(128)} %param.5) | copy-start | bytes 1540
  7.2 16.3 %all-gather.9.cloned.1.call-start = ((), (), s32[]{:S(2)}) async-start(), calls=%async_computation.5 | async-start | bytes 3145728 | tf_op jit(solution)/shard_map/all_gather | solution.py:16
  10.0 27.4 %all-gather.7.cloned.1.call-start = ((), (), s32[]{:S(2)}) async-start(), calls=%async_computation.4 | async-start | bytes 3145728 | tf_op jit(solution)/shard_map/all_gather | solution.py:15
  12.0 11.6 %copy-start.1 = (bf16[128,2048]{1,0:T(8,128)(2,1)S(1)}, bf16[128,2048]{1,0:T(8,128)(2,1)}, u32[]{:S(2)}) copy-start(bf16[128,2048]{1,0:T(8,128)(2,1)} %param.4) | copy-start | bytes 1572868
  13.1 91.3 %all-gather.11.cloned.1.call-start = ((), (), s32[]{:S(2)}) async-start(), calls=%async_computation.6 | async-start | bytes 6291456 | tf_op jit(solution)/shard_map/all_gather | solution.py:29
  23.5 148.7 %all-gather.5.cloned.1.call-start = ((), (), s32[]{:S(2)}) async-start(), calls=%async_computation.3 | async-start | bytes 4718592 | tf_op jit(solution)/shard_map/all_gather | solution.py:36
  98.7 73.5 %all-to-all-start.1 = ((bf16[2,1024,1024]{2,1,0:T(8,128)(2,1)}), bf16[2,1024,1024]{2,1,0:T(8,128)(2,1)}, u32[]{:S(2)}, u32[]{:S(2)}) async-start(bf16[2,1024,1024]{2,1,0:T(8,128)(2,1)} %pad_maximum_fusion), calls=%async_computation.1 | async-start | bytes 8388608 | tf_op jit(solution)/shard_map/all_to_all | solution.py:27
  104.3 169.3 %reduce-scatter.2.cloned.1.call-start = ((), (), s32[]{:S(2)}) async-start(), calls=%async_computation.7 | async-start | bytes 4718592 | tf_op jit(solution)/shard_map/reduce_scatter | solution.py:43
  273.6 4.8 %copy-start = (bf16[1024,2048]{1,0:T(8,128)(2,1)S(1)}, bf16[1024,2048]{1,0:T(8,128)(2,1)}, u32[]{:S(2)}) copy-start(bf16[1024,2048]{1,0:T(8,128)(2,1)} %all-gather.11.cloned.1.call-done) | copy-start | bytes 12582916
Sparse Core Ops, SparseCore 0:
  10.1 13.2 all-gather.8
  25.5 11.7 all-gather.6
  38.9 57.8 all-gather.10
  99.4 72.7 all-gather.4
  186.7 86.8 reduce-scatter.1
